TPU v7x, 32 devices: a whole 2x2x4 slice. The times are simulated.
32 devices in a mesh: ep: 4 (over y, x), tp: 8 (over z, core).
Axes of the slice: x: 2, y: 2, z: 4, core: 2. Of those that a mesh axis runs over, the one named last changes fastest.
Arguments:
- tokens: bfloat16 [2048, 2048], P('ep', 'tp'), may hold values from -6 to 6
- norm_gain: float32 [2048], replicated, may hold values from 0.1 to 1.9
- norm_shift: float32 [2048], replicated, may hold values from -3 to 3
- expert_ids: int32 [2048, 6], P('ep'), may hold values from 0 to 31, all different within a row; in each aligned block of 64 rows (0 to 63, 64 to 127, ...) at most 24 rows name the same one
- affinity: float32 [2048, 6], P('ep'), may hold values from 0.05 to 1
- expert_gate: bfloat16 [32, 2048, 512], P(('ep', 'tp')), may hold values from -0.125 to 0.125
- expert_up: bfloat16 [32, 2048, 512], P(('ep', 'tp')), may hold values from -0.125 to 0.125
- expert_down: bfloat16 [32, 512, 2048], P(('ep', 'tp')), may hold values from -0.25 to 0.25
- shared_gate: bfloat16 [512, 2048], P('tp'), may hold values from -0.125 to 0.125
- shared_up: bfloat16 [512, 2048], P('tp'), may hold values from -0.125 to 0.125
- shared_down: bfloat16 [512, 2048], replicated, may hold values from -0.25 to 0.25
Outputs:
- mixed: bfloat16 [2048, 2048], P(('ep', 'tp'))
Inputs may be any that keep to these rules, and one draw needn't show every extreme that they name: `expert_ids`: each row names 6 different experts; in each aligned block of 64 rows (the rows of one device of tp) no expert is named more than 24 times, and in some blocks an expert is named exactly 24 times.
All inputs are finite; a program needn't handle non-finite values.
Results may differ from a plain program's by a relative error of at most 0.0069.
Values may be sent and summed in bfloat16 or wider, within the bound.
A program may use at most 64 MiB of HBM per device.

v0:
```python
import jax
import jax.numpy as jnp
from jax import lax
from jax.sharding import PartitionSpec as P

ROUTED_SCALE = 2.5
EPSILON = 1e-05


def pair_ranks(flat_ids, expert_count):
    onehot = flat_ids[..., None] == jnp.arange(expert_count, dtype=jnp.int32)
    running = jnp.cumsum(onehot.astype(jnp.int32), axis=-2)
    return jnp.sum(jnp.where(onehot, running, 0), axis=-1) - 1


def expert_rows(tok_rows, w_gate, w_up, w_down):
    gate_act = jnp.dot(tok_rows, w_gate, preferred_element_type=jnp.float32)
    up_act = jnp.dot(tok_rows, w_up, preferred_element_type=jnp.float32)
    hidden = (jax.nn.silu(gate_act) * up_act).astype(jnp.bfloat16)
    return jnp.dot(hidden, w_down, preferred_element_type=jnp.float32).astype(jnp.bfloat16)


def weighted_sum(source_rows, slot_index, pair_weight, top_count):
    total = jnp.zeros((slot_index.shape[0], source_rows.shape[1]), jnp.float32)
    for column in range(top_count):
        picked = jnp.take(source_rows, slot_index[:, column], axis=0, mode="fill", fill_value=0)
        total = total + pair_weight[:, column : column + 1] * picked.astype(jnp.float32)
    return total


def on_device(
    tokens,
    norm_gain,
    norm_shift,
    expert_ids,
    affinity,
    expert_gate,
    expert_up,
    expert_down,
    shared_gate,
    shared_up,
    shared_down,
):
    ep_count = lax.axis_size("ep")
    tp_count = lax.axis_size("tp")
    tp_index = lax.axis_index("tp")
    whole = lax.all_gather(tokens, "tp", axis=1, tiled=True)
    tok_count = whole.shape[0]
    width = whole.shape[1]
    top_count = expert_ids.shape[1]
    block_rows = tok_count // tp_count
    expert_count = ep_count * tp_count
    slot_cap = max(1, 2 * block_rows * top_count // expert_count)
    slot_total = expert_count * slot_cap
    values = whole.astype(jnp.float32)
    center = values - jnp.mean(values, axis=1, keepdims=True)
    spread = jnp.mean(center * center, axis=1, keepdims=True)
    normed = (center * lax.rsqrt(spread + EPSILON) * norm_gain + norm_shift).astype(jnp.bfloat16)
    weights = affinity / jnp.sum(affinity, axis=1, keepdims=True) * ROUTED_SCALE
    contract = (((1,), (1,)), ((), ()))
    shared_g = lax.dot_general(shared_gate, normed, contract, preferred_element_type=jnp.float32)
    shared_u = lax.dot_general(shared_up, normed, contract, preferred_element_type=jnp.float32)
    shared_hidden = (jax.nn.silu(shared_g) * shared_u).astype(jnp.bfloat16)
    own_hidden = lax.all_to_all(shared_hidden, "tp", split_axis=1, concat_axis=0, tiled=True)
    shared_out = lax.dot_general(
        own_hidden, shared_down, (((0,), (0,)), ((), ())), preferred_element_type=jnp.float32
    )
    block_ids = expert_ids.reshape(tp_count, block_rows * top_count)
    ranks = pair_ranks(block_ids, expert_count)
    group_index = block_ids // tp_count
    mine = block_ids % tp_count == tp_index
    block_index = jnp.arange(tp_count, dtype=jnp.int32)[:, None]
    dest = jnp.where(mine, (group_index * tp_count + block_index) * slot_cap + ranks, slot_total)
    token_index = (
        block_index * block_rows
        + jnp.arange(block_rows * top_count, dtype=jnp.int32)[None, :] // top_count
    )
    source_row = (
        jnp.full((slot_total + 1,), tok_count, jnp.int32)
        .at[dest.reshape(-1)]
        .set(token_index.reshape(-1))[:slot_total]
    )
    outgoing = jnp.take(normed, source_row, axis=0, mode="fill", fill_value=0).reshape(
        ep_count, tp_count, slot_cap, width
    )
    incoming = lax.all_to_all(outgoing, "ep", split_axis=0, concat_axis=0, tiled=True)
    result = expert_rows(incoming.reshape(-1, width), expert_gate[0], expert_up[0], expert_down[0])
    returned = lax.all_to_all(
        result.reshape(incoming.shape), "ep", split_axis=0, concat_axis=0, tiled=True
    )
    pair_slot = dest.reshape(tok_count, top_count)
    back_rows = returned.reshape(slot_total, width)
    routed = lax.psum_scatter(
        weighted_sum(back_rows, pair_slot, weights, top_count),
        "tp",
        scatter_dimension=0,
        tiled=True,
    )
    return (routed + shared_out).astype(jnp.bfloat16)


def solution(mesh):
    placed = (
        P("ep", "tp"),
        P(),
        P(),
        P("ep", None),
        P("ep", None),
        P(("ep", "tp"), None, None),
        P(("ep", "tp"), None, None),
        P(("ep", "tp"), None, None),
        P("tp", None),
        P("tp", None),
        P(),
    )
    return jax.shard_map(
        on_device, mesh=mesh, in_specs=placed, out_specs=P(("ep", "tp"), None), check_vma=False
    )
```

profile of v0, /device:TPU:0, one launch (start us, length us, event | category | flops | bytes accessed | tf_op | source)
XLA Modules:
  0.0 271.8 jit_solution(16597467197731617035)
XLA Ops:
  6.5 0.7 all-gather.2.cloned.1.call-update
  7.3 0.9 copy.34
  8.1 0.2 eq.48
  8.3 0.2 reshape.242
  8.5 0.2 eq.52
  8.8 6.9 %reduce-window.6 = s32[8,32,3,128]{3,1,2,0:T(8,128)S(1)} reduce-window(s32[8,32,3,128]{3,1,2,0:T(8,128)S(1)} %fusion.20, s32[]{:T(128)} %constant.82.clone.1), window={size=1x1x1x128 pad=0_0x0_0x0_0x127_0}, to_apply=%region_1.0 | reduce-window | flops 12484608 | bytes 786436 | tf_op jit(solution)/shard_map/reduce-window
  15.8 0.2 slice.78
  15.9 0.2 copy.40
  16.1 0.1 fusion.29
  16.3 0.2 fusion.19
  16.5 0.1 compare_select_fusion
  16.6 11.8 %scatter_custom_fusion = s32[769]{0:T(1024)S(1)} fusion(s32[3072]{0:T(1024)S(1)} %bitcast.82, s32[3072]{0:T(1024)S(1)} %reshape.307, s32[]{:T(128)} %constant.81.clone.1), kind=kCustom, calls=%fused_computation.94 | custom fusion | bytes 3080 | tf_op jit(solution)/shard_map/scatter | solution.py:81
  28.4 0.1 slice.51
  28.5 13.8 %all-gather.2.cloned.1.call-done = bf16[512,2048]{1,0:T(8,128)(2,1)} async-done(((bf16[512,256]{1,0:T(8,128)(2,1)}), bf16[512,2048]{1,0:T(8,128)(2,1)}) %all-gather.2.cloned.1.call-update) | async-done | bytes 2097168 | tf_op jit(solution)/shard_map/all_gather | solution.py:47
  42.3 2.1 convert_reduce_fusion
  44.4 0.1 copy-done.2
  44.5 0.7 fusion.2
  45.2 2.2 fusion.5
  47.4 9.0 %gather_fusion = bf16[768,2048]{1,0:T(8,128)(2,1)} fusion(bf16[512,2048]{1,0:T(8,128)(2,1)} %fusion.5, s32[1024]{0:T(1024)S(1)} %pad_clamp_fusion.6), kind=kCustom, calls=%fused_computation.6 | custom fusion | bytes 6294528 | tf_op jit(solution)/shard_map/jit(_take)/gather | solution.py:83
  56.4 3.9 %broadcast_select_fusion = bf16[4,8,24,2048]{3,2,1,0:T(8,128)(2,1)} fusion(bf16[4,8,24,2048]{3,2,1,0:T(8,128)(2,1)} %bitcast.77, pred[4,8,24]{2,1,0:T(8,128)(4,1)S(1)} %compare_and_fusion), kind=kLoop, calls=%fused_computation.18 | loop fusion | flops 1572864 | bytes 6292224 | tf_op jit(solution)/shard_map/jit(_take)/select_n | solution.py:83
  60.3 4.9 %all-to-all-start = ((bf16[4,8,24,2048]{3,2,1,0:T(8,128)(2,1)}), bf16[4,8,24,2048]{3,2,1,0:T(8,128)(2,1)}, u32[]{:S(2)}, u32[]{:S(2)}) async-start(bf16[4,8,24,2048]{3,2,1,0:T(8,128)(2,1)} %broadcast_select_fusion), calls=%async_computation | async-start | bytes 6291456 | tf_op jit(solution)/shard_map/all_to_all | solution.py:86
  65.2 0.1 add.204
  65.3 0.2 sub.37
  65.5 0.3 fusion.26
  65.8 0.8 slice_reduce_fusion.5
  66.7 35.2 %all-to-all-done = bf16[4,8,24,2048]{3,2,1,0:T(8,128)(2,1)} async-done(((bf16[4,8,24,2048]{3,2,1,0:T(8,128)(2,1)}), bf16[4,8,24,2048]{3,2,1,0:T(8,128)(2,1)}, u32[]{:S(2)}, u32[]{:S(2)}) %all-to-all-start) | async-done | bytes 3145760 | tf_op jit(solution)/shard_map/all_to_all | solution.py:86
  101.9 5.6 %fusion.10 = f32[768,512]{1,0:T(8,128)} fusion(bf16[768,2048]{1,0:T(8,128)(2,1)} %bitcast.5, bf16[1,2048,512]{2,1,0:T(8,128)(2,1)} %param.18), kind=kOutput, calls=%fused_computation.24 | convolution fusion | flops 1610612736 | bytes 6815744 | tf_op jit(solution)/shard_map/dot_general | solution.py:17
  107.4 8.2 %convolution_convert_fusion = bf16[768,2048]{1,0:T(8,128)(2,1)} fusion(bf16[1,512,2048]{2,1,0:T(8,128)(2,1)S(1)} %copy-done, f32[768,512]{1,0:T(8,128)} %fusion.10, bf16[768,2048]{1,0:T(8,128)(2,1)} %bitcast.5, bf16[1,2048,512]{2,1,0:T(8,128)(2,1)} %param.19), kind=kOutput, calls=%fused_computation.17 | convolution fusion | flops 3225157632 | bytes 12058624 | tf_op jit(solution)/shard_map/dot_general | solution.py:20
  115.6 4.6 %all-to-all-start.1 = ((bf16[4,8,24,2048]{3,2,1,0:T(8,128)(2,1)}), bf16[4,8,24,2048]{3,2,1,0:T(8,128)(2,1)}, u32[]{:S(2)}, u32[]{:S(2)}) async-start(bf16[4,8,24,2048]{3,2,1,0:T(8,128)(2,1)} %bitcast.78), calls=%async_computation.1 | async-start | bytes 6291456 | tf_op jit(solution)/shard_map/all_to_all | solution.py:88
  120.5 35.7 %all-to-all-done.1 = bf16[4,8,24,2048]{3,2,1,0:T(8,128)(2,1)} async-done(((bf16[4,8,24,2048]{3,2,1,0:T(8,128)(2,1)}), bf16[4,8,24,2048]{3,2,1,0:T(8,128)(2,1)}, u32[]{:S(2)}, u32[]{:S(2)}) %all-to-all-start.1) | async-done | bytes 3145760 | tf_op jit(solution)/shard_map/all_to_all | solution.py:88
  156.2 7.8 %gather_fusion.6 = bf16[512,2048]{1,0:T(8,128)(2,1)} fusion(bf16[768,2048]{1,0:T(8,128)(2,1)} %bitcast.10, s32[1024]{0:T(1024)S(1)} %pad_clamp_fusion), kind=kCustom, calls=%fused_computation.5.clone | custom fusion | bytes 4196352 | tf_op jit(solution)/shard_map/jit(_take)/gather | solution.py:26
  164.0 7.5 %gather_fusion.5 = bf16[512,2048]{1,0:T(8,128)(2,1)} fusion(bf16[768,2048]{1,0:T(8,128)(2,1)} %bitcast.10, s32[1024]{0:T(1024)S(1)} %pad_clamp_fusion.1), kind=kCustom, calls=%fused_computation.4.clone | custom fusion | bytes 4196352 | tf_op jit(solution)/shard_map/jit(_take)/gather | solution.py:26
  171.6 7.5 %gather_fusion.4 = bf16[512,2048]{1,0:T(8,128)(2,1)} fusion(bf16[768,2048]{1,0:T(8,128)(2,1)} %bitcast.10, s32[1024]{0:T(1024)S(1)} %pad_clamp_fusion.2), kind=kCustom, calls=%fused_computation.3.clone | custom fusion | bytes 4196352 | tf_op jit(solution)/shard_map/jit(_take)/gather | solution.py:26
  179.1 7.5 %gather_fusion.3 = bf16[512,2048]{1,0:T(8,128)(2,1)} fusion(bf16[768,2048]{1,0:T(8,128)(2,1)} %bitcast.10, s32[1024]{0:T(1024)S(1)} %pad_clamp_fusion.3), kind=kCustom, calls=%fused_computation.2.clone | custom fusion | bytes 4196352 | tf_op jit(solution)/shard_map/jit(_take)/gather | solution.py:26
  186.6 7.5 %gather_fusion.2 = bf16[512,2048]{1,0:T(8,128)(2,1)} fusion(bf16[768,2048]{1,0:T(8,128)(2,1)} %bitcast.10, s32[1024]{0:T(1024)S(1)} %pad_clamp_fusion.4), kind=kCustom, calls=%fused_computation.1.clone | custom fusion | bytes 4196352 | tf_op jit(solution)/shard_map/jit(_take)/gather | solution.py:26
  194.1 7.8 %gather_fusion.1 = bf16[512,2048]{1,0:T(8,128)(2,1)} fusion(bf16[768,2048]{1,0:T(8,128)(2,1)} %bitcast.10, s32[1024]{0:T(1024)S(1)} %pad_clamp_fusion.5), kind=kCustom, calls=%fused_computation.clone | custom fusion | bytes 4196352 | tf_op jit(solution)/shard_map/jit(_take)/gather | solution.py:26
  202.0 9.0 %multiply_add_fusion = f32[512,2048]{1,0:T(8,128)} fusion(bf16[512,2048]{1,0:T(8,128)(2,1)} %gather_fusion.6, bf16[512,2048]{1,0:T(8,128)(2,1)} %gather_fusion.5, bf16[512,2048]{1,0:T(8,128)(2,1)} %gather_fusion.4, bf16[512,2048]{1,0:T(8,128)(2,1)} %gather_fusion.3, bf16[512,2048]{1,0:T(8,128)(2,1)} %gather_fusion.2, bf16[512,2048]{1,0:T(8,128)(2,1)} %gather_fusion.1, ...), kind=kLoop, calls=%fused_computation.16 | loop fusion | flops 24117248 | bytes 16792576 | tf_op jit(solution)/shard_map/add | solution.py:27
  211.1 0.9 copy-done.3
  212.0 2.5 convolution_bitcast_fusion.1
  214.5 0.8 fusion.15
  215.3 0.1 copy.46
  215.4 0.2 reshape.338
  215.6 11.3 %all_to_all.29 = bf16[8,2,2048]{2,1,0:T(2,128)(2,1)S(1)} all-to-all(bf16[8,2,2048]{2,1,0:T(2,128)(2,1)S(1)} %reshape.338), channel_id=1, replica_groups=mesh['ep'=4,'tp'=8] {'tp'}, dimensions={0} | all-to-all | bytes 131072 | tf_op jit(solution)/shard_map/all_to_all | solution.py:64
  226.9 0.1 reshape.339
  227.0 0.1 copy.45
  227.1 0.1 all_to_all.25
  227.3 34.9 %reduce-scatter.2.cloned.1.call-done = f32[64,2048]{1,0:T(8,128)} async-done(((f32[512,2048]{1,0:T(8,128)}), f32[64,2048]{1,0:T(8,128)}) %reduce-scatter.2.cloned.1.call-update) | async-done | bytes 524304 | tf_op jit(solution)/shard_map/reduce_scatter | solution.py:93
  262.1 2.9 %fusion.6 = bf16[64,2048]{1,0:T(8,128)(2,1)} fusion(f32[64,2048]{1,0:T(8,128)} %reduce-scatter.2.cloned.1.call-done, bf16[512,64]{0,1:T(8,128)(2,1)S(1)} %all_to_all.25, bf16[512,2048]{1,0:T(8,128)(2,1)} %param.23), kind=kOutput, calls=%fused_computation.20 | convolution fusion | flops 134479872 | bytes 2949120 | tf_op jit(solution)/shard_map/dot_general | solution.py:65
  (50 shorter events, 0.4 us)
Async XLA Ops:
  6.5 100.9 %copy-start = (bf16[1,512,2048]{2,1,0:T(8,128)(2,1)S(1)}, bf16[1,512,2048]{2,1,0:T(8,128)(2,1)}, u32[]{:S(2)}) copy-start(bf16[1,512,2048]{2,1,0:T(8,128)(2,1)} %param.20) | copy-start | bytes 6291460
  6.5 35.8 %all-gather.2.cloned.1.call-start = ((), (), s32[]{:S(2)}) async-start(), calls=%async_computation.4 | async-start | bytes 2359296 | tf_op jit(solution)/shard_map/all_gather | solution.py:47
  42.3 2.2 copy-start.2
  42.3 2.9 %copy-start.5 = (f32[2048]{0:T(1024)S(1)}, f32[2048]{0:T(1024)}, u32[]{:S(2)}) copy-start(f32[2048]{0:T(1024)} %param.15) | copy-start | bytes 24580
  42.3 2.9 %copy-start.6 = (f32[2048]{0:T(1024)S(1)}, f32[2048]{0:T(1024)}, u32[]{:S(2)}) copy-start(f32[2048]{0:T(1024)} %param.14) | copy-start | bytes 24580
  60.3 5.3 %copy-start.4 = (f32[512,6]{0,1:T(8,128)S(1)}, f32[512,6]{0,1:T(8,128)}, u32[]{:S(2)}) copy-start(f32[512,6]{0,1:T(8,128)} %param.17) | copy-start | bytes 36868
  60.3 41.6 %all-to-all-start = ((bf16[4,8,24,2048]{3,2,1,0:T(8,128)(2,1)}), bf16[4,8,24,2048]{3,2,1,0:T(8,128)(2,1)}, u32[]{:S(2)}, u32[]{:S(2)}) async-start(bf16[4,8,24,2048]{3,2,1,0:T(8,128)(2,1)} %broadcast_select_fusion), calls=%async_computation | async-start | bytes 6291456 | tf_op jit(solution)/shard_map/all_to_all | solution.py:86
  115.6 40.6 %all-to-all-start.1 = ((bf16[4,8,24,2048]{3,2,1,0:T(8,128)(2,1)}), bf16[4,8,24,2048]{3,2,1,0:T(8,128)(2,1)}, u32[]{:S(2)}, u32[]{:S(2)}) async-start(bf16[4,8,24,2048]{3,2,1,0:T(8,128)(2,1)} %bitcast.78), calls=%async_computation.1 | async-start | bytes 6291456 | tf_op jit(solution)/shard_map/all_to_all | solution.py:88
  120.3 141.9 %reduce-scatter.2.cloned.1.call-start = ((), (), s32[]{:S(2)}) async-start(), calls=%async_computation.5 | async-start | bytes 4718592 | tf_op jit(solution)/shard_map/reduce_scatter | solution.py:93
  211.0 0.9 copy-start.3
  212.0 2.5 copy-start.1
  212.0 2.5 copy-start.7
Sparse Core Ops, SparseCore 0:
  8.9 33.3 all-gather.1
  211.2 50.8 reduce-scatter.1
where the time goes:
time: 273 us; the launch traced here: 272 us
  waiting for transfers between devices  120 us (44%)
  local copies, waits for them, and re-layouts  71.2 us (26%)
  other arithmetic  25.8 us (9%)
  matrix products  19.9 us (7%)
  between operations  13.8 us (5%)
  blocking collectives  11.3 us (4%)
  starting transfers between devices  9.63 us (4%)
    gather x6, local copies, waits for them, and re-layouts, weighted_sum(): jnp.take(source_rows, slot_index[:, column], axis=0, mode='fill', fill_va...  45.7 us
    all_to_all x1, waiting for transfers between devices, on_device(): lax.all_to_all(result.reshape(incoming.shape), 'ep', split_axis=0, concat...  35.7 us
    all_to_all x1, waiting for transfers between devices, on_device(): lax.all_to_all(outgoing, 'ep', split_axis=0, concat_axis=0, tiled=True)  35.2 us
    reduce_scatter x1, waiting for transfers between devices, on_device(): lax.psum_scatter(weighted_sum(back_rows, pair_slot, weights, top_count),...  34.9 us
    all_gather x1, waiting for transfers between devices, on_device(): whole = lax.all_gather(tokens, 'tp', axis=1, tiled=True)  13.8 us
    scatter x1, local copies, waits for them, and re-layouts, on_device(): source_row = jnp.full((slot_total + 1,), tok_count, jnp.int32).at[dest.re...  11.8 us
    all_to_all x1, blocking collectives, on_device(): lax.all_to_all(shared_hidden, 'tp', split_axis=1, concat_axis=0, tiled=True)  11.3 us
    add x1, other arithmetic, weighted_sum(): total + pair_weight[:, column:column + 1] * picked.astype(jnp.float32)  9.05 us
  transfers between devices with their start and end apart: 4, of which 4 were waited for; matrix products, arithmetic and copies ran while one was open for 10% of the time, Pallas kernels for 0%

commit v1 on v0

v1 whole, which is shorter than its diff:
```python
import jax
import jax.numpy as jnp
from jax import lax
from jax.sharding import PartitionSpec as P

ROUTED_SCALE = 2.5
EPSILON = 1e-05


def expert_rows(tok_rows, w_gate, w_up, w_down):
    gate_act = jnp.dot(tok_rows, w_gate, preferred_element_type=jnp.float32)
    up_act = jnp.dot(tok_rows, w_up, preferred_element_type=jnp.float32)
    hidden = (jax.nn.silu(gate_act) * up_act).astype(jnp.bfloat16)
    return jnp.dot(hidden, w_down, preferred_element_type=jnp.float32).astype(jnp.bfloat16)


def on_device(
    tokens,
    norm_gain,
    norm_shift,
    expert_ids,
    affinity,
    expert_gate,
    expert_up,
    expert_down,
    shared_gate,
    shared_up,
    shared_down,
):
    ep_count = lax.axis_size("ep")
    tp_count = lax.axis_size("tp")
    tp_index = lax.axis_index("tp")
    whole = lax.all_gather(tokens, "tp", axis=1, tiled=True)
    tok_count = whole.shape[0]
    width = whole.shape[1]
    top_count = expert_ids.shape[1]
    block_rows = tok_count // tp_count
    expert_count = ep_count * tp_count
    slot_cap = max(1, 2 * block_rows * top_count // expert_count)
    slot_total = expert_count * slot_cap
    values = whole.astype(jnp.float32)
    center = values - jnp.mean(values, axis=1, keepdims=True)
    spread = jnp.mean(center * center, axis=1, keepdims=True)
    normed = (center * lax.rsqrt(spread + EPSILON) * norm_gain + norm_shift).astype(jnp.bfloat16)
    weights = affinity / jnp.sum(affinity, axis=1, keepdims=True) * ROUTED_SCALE
    contract = (((1,), (1,)), ((), ()))
    shared_g = lax.dot_general(shared_gate, normed, contract, preferred_element_type=jnp.float32)
    shared_u = lax.dot_general(shared_up, normed, contract, preferred_element_type=jnp.float32)
    shared_hidden = (jax.nn.silu(shared_g) * shared_u).astype(jnp.bfloat16)
    down_part = lax.dynamic_slice_in_dim(
        shared_down, tp_index * shared_gate.shape[0], shared_gate.shape[0], axis=0
    )
    experts = jnp.arange(ep_count, dtype=jnp.int32) * tp_count + tp_index
    hits = expert_ids[:, None, :] == experts[None, :, None]
    chosen = jnp.any(hits, axis=2)
    pair_weight = jnp.sum(jnp.where(hits, weights[:, None, :], 0), axis=2)
    rows = jnp.arange(tok_count, dtype=jnp.int32)
    before = (rows[:, None] > rows[None, :]) & (
        rows[:, None] // block_rows == rows[None, :] // block_rows
    )
    ranks = jnp.dot(
        before.astype(jnp.bfloat16), chosen.astype(jnp.bfloat16), preferred_element_type=jnp.float32
    ).astype(jnp.int32)
    place = jnp.where(chosen, (rows // block_rows)[:, None] * slot_cap + ranks, -1)
    slots = jnp.arange(tp_count * slot_cap, dtype=jnp.int32)
    pick = (place.T[:, None, :] == slots[None, :, None]).astype(jnp.bfloat16)
    outgoing = jnp.dot(
        pick.reshape(slot_total, tok_count), normed, preferred_element_type=jnp.float32
    ).astype(jnp.bfloat16)
    outgoing = outgoing.reshape(ep_count, tp_count * slot_cap, width)
    incoming = lax.all_to_all(outgoing, "ep", split_axis=0, concat_axis=0, tiled=True)
    result = expert_rows(incoming.reshape(-1, width), expert_gate[0], expert_up[0], expert_down[0])
    returned = lax.all_to_all(
        result.reshape(incoming.shape), "ep", split_axis=0, concat_axis=0, tiled=True
    )
    spread_weight = jnp.where(
        place[:, :, None] == slots[None, None, :], pair_weight[:, :, None], 0
    ).reshape(tok_count, slot_total).astype(jnp.bfloat16)
    part = jnp.dot(
        spread_weight, returned.reshape(slot_total, width), preferred_element_type=jnp.float32
    ) + lax.dot_general(
        shared_hidden, down_part, (((0,), (0,)), ((), ())), preferred_element_type=jnp.float32
    )
    total = lax.psum_scatter(part.astype(jnp.bfloat16), "tp", scatter_dimension=0, tiled=True)
    return total.astype(jnp.bfloat16)


def solution(mesh):
    placed = (
        P("ep", "tp"),
        P(),
        P(),
        P("ep", None),
        P("ep", None),
        P(("ep", "tp"), None, None),
        P(("ep", "tp"), None, None),
        P(("ep", "tp"), None, None),
        P("tp", None),
        P("tp", None),
        P(),
    )
    return jax.shard_map(
        on_device, mesh=mesh, in_specs=placed, out_specs=P(("ep", "tp"), None), check_vma=False
    )
```

time: 273 us -> 196 us (0.72)
  local copies, waits for them, and re-layouts: 71.2 us -> 1.9 us
  blocking collectives: 11.3 us -> 40.5 us
  other arithmetic: 25.8 us -> 4.86 us
  waiting for transfers between devices: 120 us -> 103 us
  matrix products: 19.9 us -> 27.1 us
  starting transfers between devices: 9.63 us -> 4.81 us
    gather x7 -> x0, local copies, waits for them, and re-layouts: 54.7 us -> none  [the longest x6 45.7 us: weighted_sum(): jnp.take(source_rows, slot_index[:, column], axis=0, mode='fill', fill_va...]
    all_to_all x1 -> x0, waiting for transfers between devices: 35.2 us -> none  [on_device(): lax.all_to_all(outgoing, 'ep', split_axis=0, concat_axis=0, tiled=True)]
    all_to_all x1, blocking collectives: 11.3 us -> 40.5 us  [on_device(): lax.all_to_all(outgoing, 'ep', split_axis=0, concat_axis=0, tiled=True)]
    all_gather x1, waiting for transfers between devices: 13.8 us -> 33.5 us  [on_device(): whole = lax.all_gather(tokens, 'tp', axis=1, tiled=True)]
    scatter x1 -> x0, local copies, waits for them, and re-layouts: 11.8 us -> none  [on_device(): source_row = jnp.full((slot_total + 1,), tok_count, jnp.int32).at[dest.re...]
    dot_general x2 -> x4, matrix products: 3.62 us -> 13.6 us  [the longest x1 5.75 us: on_device(): lax.dot_general(shared_hidden, down_part, (((0,), (0,)), ((), ())), prefe...]
    add x2 -> x1, other arithmetic: 9.12 us -> 0.01 us  [on_device(): experts = jnp.arange(ep_count, dtype=jnp.int32) * tp_count + tp_index]
    another operation x2 -> x0, other arithmetic: 7.02 us -> none
  transfers between devices with their start and end apart: 4 -> 3, of which waited for: 4 -> 3; matrix products, arithmetic and copies ran while one was open for 10% -> 2% of each run, Pallas kernels for 0% -> 0%
where the time goes in v1:
time: 196 us
  waiting for transfers between devices  103 us (53%)
  blocking collectives  40.5 us (21%)
  matrix products  27.1 us (14%)
  between operations  13.5 us (7%)
  other arithmetic  4.86 us (2%)
  starting transfers between devices  4.81 us (2%)
    all_to_all x1, blocking collectives, on_device(): lax.all_to_all(outgoing, 'ep', split_axis=0, concat_axis=0, tiled=True)  40.5 us
    reduce_scatter x1, waiting for transfers between devices, on_device(): lax.psum_scatter(part.astype(jnp.bfloat16), 'tp', scatter_dimension=0, ti...  35.9 us
    all_gather x1, waiting for transfers between devices, on_device(): whole = lax.all_gather(tokens, 'tp', axis=1, tiled=True)  33.5 us
    all_to_all x1, waiting for transfers between devices, on_device(): lax.all_to_all(result.reshape(incoming.shape), 'ep', split_axis=0, concat...  32.8 us
    dot_general x1, matrix products, expert_rows(): jnp.dot(hidden, w_down, preferred_element_type=jnp.float32)  8.15 us
    dot_general x1, matrix products, on_device(): lax.dot_general(shared_hidden, down_part, (((0,), (0,)), ((), ())), prefe...  5.75 us
    dot_general x1, matrix products, on_device(): jnp.dot(spread_weight, returned.reshape(slot_total, width), preferred_ele...  5.75 us
    all_to_all x1, starting transfers between devices, on_device(): lax.all_to_all(result.reshape(incoming.shape), 'ep', split_axis=0, concat...  4.77 us
  transfers between devices with their start and end apart: 3, of which 3 were waited for; matrix products, arithmetic and copies ran while one was open for 2% of the time, Pallas kernels for 0%

profile of v1, /device:TPU:0, one launch (start us, length us, event | category | flops | bytes accessed | tf_op | source)
XLA Modules:
  0.0 195.7 jit_solution(381169788603130754)
XLA Ops:
  6.5 0.0 copy-start
  6.5 0.0 all-gather.2.cloned.1.call-start
  6.5 0.7 all-gather.2.cloned.1.call-update
  7.3 0.1 eq.73
  7.4 0.8 compare_reduce_fusion
  8.2 0.3 fusion.17
  8.5 0.3 bitcast_compare_fusion
  8.8 33.5 %all-gather.2.cloned.1.call-done = bf16[512,2048]{1,0:T(8,128)(2,1)} async-done(((bf16[512,256]{1,0:T(8,128)(2,1)}), bf16[512,2048]{1,0:T(8,128)(2,1)}) %all-gather.2.cloned.1.call-update) | async-done | bytes 2097168 | tf_op jit(solution)/shard_map/all_gather | solution.py:33
  42.3 0.0 copy-start.2
  42.3 0.0 copy-start.8
  42.3 0.0 copy-start.9
  42.3 2.1 %convert_reduce_fusion = f32[512]{0:T(512)S(1)} fusion(bf16[512,2048]{1,0:T(8,128)(2,1)} %all-gather.2.cloned.1.call-done), kind=kLoop, calls=%fused_computation.1 | loop fusion | flops 2096640 | bytes 2099200 | tf_op jit(solution)/shard_map/reduce_sum | solution.py:42
  44.4 0.1 copy-done.2
  44.5 0.7 fusion.2
  45.2 0.0 copy-done.8
  45.2 0.0 copy-done.9
  45.2 0.8 fusion.5
  46.1 0.0 copy-start.1
  46.1 1.8 convolution_convert_fusion.1
  47.9 0.0 copy-done.1
  47.9 0.0 copy-start.10
  47.9 40.5 %all_to_all.10 = bf16[4,192,2048]{2,1,0:T(8,128)(2,1)S(1)} all-to-all(bf16[4,192,2048]{2,1,0:T(8,128)(2,1)S(1)} %bitcast.46), channel_id=1, replica_groups=mesh['ep'=4,'tp'=8] {'ep'}, dimensions={0} | all-to-all | bytes 6291456 | tf_op jit(solution)/shard_map/all_to_all | solution.py:71
  88.5 0.0 copy-start.3
  88.5 1.7 copy-done.3
  90.1 0.0 copy-done.10
  90.1 3.0 %fusion.10 = f32[768,512]{1,0:T(8,128)} fusion(bf16[768,2048]{1,0:T(8,128)(2,1)S(1)} %bitcast.44, bf16[1,2048,512]{2,1,0:T(8,128)(2,1)S(1)} %copy-done.10), kind=kOutput, calls=%fused_computation.15 | convolution fusion | flops 1610612736 | bytes 6815744 | tf_op jit(solution)/shard_map/dot_general | solution.py:11
  93.1 0.0 copy-done
  93.1 8.1 %convolution_convert_fusion = bf16[768,2048]{1,0:T(8,128)(2,1)} fusion(bf16[1,512,2048]{2,1,0:T(8,128)(2,1)S(1)} %copy-done, f32[768,512]{1,0:T(8,128)} %fusion.10, bf16[768,2048]{1,0:T(8,128)(2,1)} %bitcast.45, bf16[1,2048,512]{2,1,0:T(8,128)(2,1)} %param.17), kind=kOutput, calls=%fused_computation.10 | convolution fusion | flops 3225157632 | bytes 12058624 | tf_op jit(solution)/shard_map/dot_general | solution.py:14
  101.3 0.0 copy-start.7
  101.3 0.0 copy-start.6
  101.3 0.0 copy-start.4
  101.3 4.8 %all-to-all-start.1 = ((bf16[4,192,2048]{2,1,0:T(8,128)(2,1)}), bf16[4,192,2048]{2,1,0:T(8,128)(2,1)}, u32[]{:S(2)}, u32[]{:S(2)}) async-start(bf16[4,192,2048]{2,1,0:T(8,128)(2,1)} %bitcast.43), calls=%async_computation.1 | async-start | bytes 6291456 | tf_op jit(solution)/shard_map/all_to_all | solution.py:73
  106.1 0.0 reduce-scatter.2.cloned.1.call-start
  106.1 0.0 copy-done.7
  106.2 0.0 copy-done.6
  106.2 0.1 fusion.36
  106.3 0.0 copy-done.4
  106.3 2.4 %convolution_bitcast_fusion.1 = f32[64,512]{1,0:T(8,128)S(1)} fusion(bf16[512,2048]{1,0:T(8,128)(2,1)} %copy-done.1, bf16[64,2048]{1,0:T(8,128)(2,1)S(1)} %copy-done.4), kind=kOutput, calls=%fused_computation.23 | convolution fusion | flops 134217728 | bytes 2490368 | tf_op jit(solution)/shard_map/dot_general | solution.py:47
  108.6 0.0 copy-start.5
  108.6 32.8 %all-to-all-done.1 = bf16[4,192,2048]{2,1,0:T(8,128)(2,1)} async-done(((bf16[4,192,2048]{2,1,0:T(8,128)(2,1)}), bf16[4,192,2048]{2,1,0:T(8,128)(2,1)}, u32[]{:S(2)}, u32[]{:S(2)}) %all-to-all-start.1) | async-done | bytes 3145760 | tf_op jit(solution)/shard_map/all_to_all | solution.py:73
  141.4 5.7 %fusion.21 = f32[512,2048,1]{1,0,2:T(8,128)} fusion(bf16[4,192,2048]{2,1,0:T(8,128)(2,1)} %all-to-all-done.1, bf16[512,4]{0,1:T(4,128)(2,1)S(1)} %fusion.36, s32[512,4]{0,1:T(4,128)S(1)} %fusion.17), kind=kOutput, calls=%fused_computation.31 | convolution fusion | flops 1611399168 | bytes 7352320 | tf_op jit(solution)/shard_map/dot_general | solution.py:79
  147.2 0.0 copy-done.5
  147.2 5.8 %fusion.6 = bf16[512,2048]{1,0:T(8,128)(2,1)} fusion(f32[512,2048,1]{1,0,2:T(8,128)} %fusion.21, bf16[512,2048]{1,0:T(8,128)(2,1)} %copy-done.1, bf16[64,2048]{1,0:T(8,128)(2,1)S(1)} %copy-done.5, bf16[512,2048]{1,0:T(8,128)(2,1)} %param.21, s32[]{:T(128)S(6)} %select_n.52, f32[64,512]{1,0:T(8,128)S(1)} %convolution_bitcast_fusion.1), kind=kOutput, calls=%fused_computation.9 | convolution fusion | flops 270729216 | bytes 9043972 | tf_op jit(solution)/shard_map/dot_general | solution.py:81
  152.9 0.0 reduce-scatter.2.cloned.1.call-update
  153.0 35.9 %reduce-scatter.2.cloned.1.call-done = bf16[64,2048]{1,0:T(8,128)(2,1)} async-done(((bf16[512,2048]{1,0:T(8,128)(2,1)}), bf16[64,2048]{1,0:T(8,128)(2,1)}) %reduce-scatter.2.cloned.1.call-update) | async-done | bytes 262160 | tf_op jit(solution)/shard_map/reduce_scatter | solution.py:84
  (7 shorter events, 0.1 us)
Async XLA Ops:
  6.5 86.6 %copy-start = (bf16[1,512,2048]{2,1,0:T(8,128)(2,1)S(1)}, bf16[1,512,2048]{2,1,0:T(8,128)(2,1)}, u32[]{:S(2)}) copy-start(bf16[1,512,2048]{2,1,0:T(8,128)(2,1)} %param.18) | copy-start | bytes 6291460
  6.5 35.8 %all-gather.2.cloned.1.call-start = ((), (), s32[]{:S(2)}) async-start(), calls=%async_computation.3 | async-start | bytes 2359296 | tf_op jit(solution)/shard_map/all_gather | solution.py:33
  42.3 2.2 %copy-start.2 = (bf16[512,2048]{1,0:T(8,128)(2,1)S(1)}, bf16[512,2048]{1,0:T(8,128)(2,1)}, u32[]{:S(2)}) copy-start(bf16[512,2048]{1,0:T(8,128)(2,1)} %all-gather.2.cloned.1.call-done) | copy-start | bytes 6291460
  42.3 2.9 %copy-start.8 = (f32[2048]{0:T(1024)S(1)}, f32[2048]{0:T(1024)}, u32[]{:S(2)}) copy-start(f32[2048]{0:T(1024)} %param.13) | copy-start | bytes 24580
  42.3 2.9 %copy-start.9 = (f32[2048]{0:T(1024)S(1)}, f32[2048]{0:T(1024)}, u32[]{:S(2)}) copy-start(f32[2048]{0:T(1024)} %param.12) | copy-start | bytes 24580
  46.1 1.8 copy-start.1
  47.9 42.2 %copy-start.10 = (bf16[1,2048,512]{2,1,0:T(8,128)(2,1)S(1)}, bf16[1,2048,512]{2,1,0:T(8,128)(2,1)}, u32[]{:S(2)}) copy-start(bf16[1,2048,512]{2,1,0:T(8,128)(2,1)} %param.16) | copy-start | bytes 6291460
  88.5 1.7 copy-start.3
  101.3 4.8 %copy-start.7 = (f32[512,6]{0,1:T(8,128)S(1)}, f32[512,6]{0,1:T(8,128)}, u32[]{:S(2)}) copy-start(f32[512,6]{0,1:T(8,128)} %param.15) | copy-start | bytes 36868
  101.3 4.9 %copy-start.6 = (s32[512,6]{0,1:T(8,128)S(1)}, s32[512,6]{0,1:T(8,128)}, u32[]{:S(2)}) copy-start(s32[512,6]{0,1:T(8,128)} %param.14) | copy-start | bytes 36868
  101.3 5.0 %copy-start.4 = (bf16[64,2048]{1,0:T(8,128)(2,1)S(1)}, bf16[64,2048]{1,0:T(8,128)(2,1)}, u32[]{:S(2)}) copy-start(bf16[64,2048]{1,0:T(8,128)(2,1)} %param.19) | copy-start | bytes 786436
  101.3 40.1 %all-to-all-start.1 = ((bf16[4,192,2048]{2,1,0:T(8,128)(2,1)}), bf16[4,192,2048]{2,1,0:T(8,128)(2,1)}, u32[]{:S(2)}, u32[]{:S(2)}) async-start(bf16[4,192,2048]{2,1,0:T(8,128)(2,1)} %bitcast.43), calls=%async_computation.1 | async-start | bytes 6291456 | tf_op jit(solution)/shard_map/all_to_all | solution.py:73
  106.1 82.8 %reduce-scatter.2.cloned.1.call-start = ((), (), s32[]{:S(2)}) async-start(), calls=%async_computation.4 | async-start | bytes 2359296 | tf_op jit(solution)/shard_map/reduce_scatter | solution.py:84
  108.6 38.6 %copy-start.5 = (bf16[64,2048]{1,0:T(8,128)(2,1)S(1)}, bf16[64,2048]{1,0:T(8,128)(2,1)}, u32[]{:S(2)}) copy-start(bf16[64,2048]{1,0:T(8,128)(2,1)} %param.20) | copy-start | bytes 786436
Sparse Core Ops, SparseCore 0:
  8.9 33.3 all-gather.1
  153.1 35.7 reduce-scatter.1

commit v2 on v1

v2 whole, which is shorter than its diff:
```python
import functools
import math

import jax
import jax.numpy as jnp
from jax import lax
from jax.experimental import pallas as pl
from jax.experimental.pallas import tpu as pltpu
from jax.sharding import PartitionSpec as P

ROUTED_SCALE = 2.5
EPSILON = 1e-05
MESH = pl.DeviceIdType.MESH
F32 = jnp.float32
BF16 = jnp.bfloat16


def layer_kernel(
    sizes,
    tokens_ref,
    slot_ref,
    slot_t_ref,
    weight_ref,
    gain_ref,
    shift_ref,
    sgate_ref,
    sup_ref,
    gate_hbm,
    up_hbm,
    down_hbm,
    sdown_hbm,
    out_ref,
    gate_ref,
    up_ref,
    down_ref,
    sdown_ref,
    whole,
    pick,
    spread,
    sent,
    inc,
    norm,
    hidden,
    shidden,
    res,
    ret,
    part,
    own,
    pair_out,
    pair_in,
    far_out,
    far_in,
    load_sem,
    a_send,
    f_send,
    a_recv,
    b_send,
    b_recv,
    r_send,
    r_recv,
    p_send,
    p_recv,
    q_send,
    q_recv,
):
    ep, tp, rows, slots, feat, chunks, cols = sizes
    chips = tp // 2
    g = lax.axis_index("ep")
    t = lax.axis_index("tp")
    z = t // 2
    c = t % 2
    mate = z * 2 + 1 - c
    width = tp * feat
    shared_rows = sdown_ref.shape[0]

    loads = [
        pltpu.make_async_copy(gate_hbm, gate_ref, load_sem.at[0]),
        pltpu.make_async_copy(up_hbm, up_ref, load_sem.at[1]),
        pltpu.make_async_copy(down_hbm, down_ref, load_sem.at[2]),
        pltpu.make_async_copy(
            sdown_hbm.at[pl.ds(pl.multiple_of(t * shared_rows, 8), shared_rows)],
            sdown_ref,
            load_sem.at[3],
        ),
    ]
    for load in loads:
        load.start()

    def remote(src, dst, send, recv, e, k):
        return pltpu.make_async_remote_copy(
            src_ref=src,
            dst_ref=dst,
            send_sem=send,
            recv_sem=recv,
            device_id=(e, k),
            device_id_type=MESH,
        )

    barrier = pltpu.get_barrier_semaphore()
    partners = [(lax.rem(g + p, ep), t) for p in range(1, ep)]
    partners += [(g, lax.rem(z + d, chips) * 2 + c) for d in range(1, chips)]
    partners += [(g, mate)]
    for e, k in partners:
        pl.semaphore_signal(barrier, inc=1, device_id=(e, k), device_id_type=MESH)
    pl.semaphore_wait(barrier, len(partners))

    first = []
    first.append(remote(tokens_ref, whole.at[t], f_send.at[0], a_recv.at[t], g, mate))
    for d in range(1, chips):
        there = lax.rem(z + d, chips) * 2 + c
        first.append(remote(tokens_ref, whole.at[t], a_send.at[d], a_recv.at[t], g, there))
    for copy in first:
        copy.start()
    whole[t] = tokens_ref[...]

    for e in range(ep):
        line = lax.broadcasted_iota(jnp.int32, (slots, rows), 0) + e * slots
        pick[e] = jnp.where(line == slot_t_ref[e : e + 1, :], 1.0, 0.0).astype(BF16)
    line = lax.broadcasted_iota(jnp.int32, (rows, ep * slots), 1)
    mixed = jnp.zeros((rows, ep * slots), F32)
    for e in range(ep):
        mixed = jnp.where(line == slot_ref[:, e : e + 1], weight_ref[:, e : e + 1], mixed)
    spread[...] = mixed.astype(BF16)

    def forward(k, d):
        return remote(whole.at[k], whole.at[k], f_send.at[d], a_recv.at[k], g, mate)

    def chunk_step(i, carry):
        d = i // 2
        side = i % 2
        zz = lax.rem(z + d, chips)
        k = zz * 2 + lax.rem(c + side, 2)

        @pl.when(i > 0)
        def _():
            forward(k, d).wait_recv()

        @pl.when((i > 0) & (side == 0))
        def _():
            forward(k, d).start()

        picked = jnp.dot(
            pick[...].reshape(ep * slots, rows), whole[k], preferred_element_type=F32
        ).astype(BF16)
        sent[k] = picked.reshape(ep, slots, feat)
        inc[k, g] = sent[k, g]
        for p in range(1, ep):
            e = lax.rem(g + p, ep)
            remote(
                sent.at[k, e], inc.at[k, g], b_send.at[k, e], b_recv.at[k, g], e, t
            ).start()
        return carry

    lax.fori_loop(0, tp, chunk_step, 0)

    def normalise(read, count):
        tile = math.gcd(64, count)

        def body(i, carry):
            at = pl.ds(pl.multiple_of(i * tile, tile), tile)
            total = jnp.zeros((tile, feat), F32)
            for k in range(tp):
                total = total + read(k, at).astype(F32)
            mean = jnp.sum(total, axis=1, keepdims=True) / width
            total = jnp.zeros((tile, feat), F32)
            for k in range(tp):
                center = read(k, at).astype(F32) - mean
                total = total + center * center
            scale = lax.rsqrt(jnp.sum(total, axis=1, keepdims=True) / width + EPSILON)
            for k in range(tp):
                lanes = slice(k * feat, (k + 1) * feat)
                value = (read(k, at).astype(F32) - mean) * scale
                value = value * gain_ref[:, lanes] + shift_ref[:, lanes]
                norm[at, lanes] = value.astype(BF16)
            return carry

        lax.fori_loop(0, count // tile, body, 0)

    normalise(lambda k, at: whole[k, at, :], rows)
    contract = (((1,), (1,)), ((), ()))
    sg = lax.dot_general(norm[...], sgate_ref[...], contract, preferred_element_type=F32)
    su = lax.dot_general(norm[...], sup_ref[...], contract, preferred_element_type=F32)
    shidden[...] = (jax.nn.silu(sg) * su).astype(BF16)

    for load in loads:
        load.wait()

    def expert_step(p, carry):
        s = lax.rem(g + p, ep)

        @pl.when(p > 0)
        def _():
            for k in range(tp):
                remote(
                    sent.at[k, s], inc.at[k, s], b_send.at[k, s], b_recv.at[k, s], s, t
                ).wait_recv()

        normalise(lambda k, at: inc[k, s, at, :], slots)
        got = norm[0:slots, :]
        gate_act = jnp.dot(got, gate_ref[...], preferred_element_type=F32)
        up_act = jnp.dot(got, up_ref[...], preferred_element_type=F32)
        hidden[s] = (jax.nn.silu(gate_act) * up_act).astype(BF16)
        return carry

    lax.fori_loop(0, ep, expert_step, 0)

    def lanes_of(i):
        return pl.ds(pl.multiple_of(i * cols, cols), cols)

    def down_step(i, carry):
        rows_out = jnp.dot(
            hidden[...].reshape(ep * slots, hidden.shape[2]),
            down_ref[:, lanes_of(i)],
            preferred_element_type=F32,
        ).astype(BF16)
        res[i] = rows_out.reshape(ep, slots, cols)
        ret[i, g] = res[i, g]
        for p in range(1, ep):
            e = lax.rem(g + p, ep)
            remote(
                res.at[i, e], ret.at[i, g], r_send.at[i, e], r_recv.at[i, g], e, t
            ).start()
        return carry

    lax.fori_loop(0, chunks, down_step, 0)

    def pair_copy(i):
        return remote(pair_out.at[i], pair_in.at[i], p_send.at[i], p_recv.at[i], g, mate)

    def sum_step(i, carry):
        for p in range(1, ep):
            s = lax.rem(g + p, ep)
            remote(
                res.at[i, s], ret.at[i, s], r_send.at[i, s], r_recv.at[i, s], s, t
            ).wait_recv()
        total = jnp.dot(
            spread[...], ret[i].reshape(ep * slots, cols), preferred_element_type=F32
        ) + jnp.dot(shidden[...], sdown_ref[:, lanes_of(i)], preferred_element_type=F32)
        part[...] = total.reshape(part.shape)
        for zz in range(chips):
            pair_out[i, zz] = part[zz * 2 + 1 - c].astype(BF16)
        pair_copy(i).start()
        pair_copy(i).wait_recv()
        own[i] = part[t] + pair_in[i, z].astype(F32)
        for d in range(1, chips):
            zz = lax.rem(z + d, chips)
            far_out[i, zz] = (part[zz * 2 + c] + pair_in[i, zz].astype(F32)).astype(BF16)
            remote(
                far_out.at[i, zz],
                far_in.at[i, z],
                q_send.at[i, zz],
                q_recv.at[i, z],
                g,
                zz * 2 + c,
            ).start()
        return carry

    lax.fori_loop(0, chunks, sum_step, 0)

    def out_step(i, carry):
        total = own[i]
        for d in range(1, chips):
            zz = lax.rem(z + d, chips)
            remote(
                far_out.at[i, zz],
                far_in.at[i, zz],
                q_send.at[i, zz],
                q_recv.at[i, zz],
                g,
                zz * 2 + c,
            ).wait()
            total = total + far_in[i, zz].astype(F32)
        out_ref[:, lanes_of(i)] = total.astype(BF16)
        pair_copy(i).wait_send()
        for p in range(1, ep):
            e = lax.rem(g + p, ep)
            remote(
                res.at[i, e], ret.at[i, e], r_send.at[i, e], r_recv.at[i, e], e, t
            ).wait_send()
        return carry

    lax.fori_loop(0, chunks, out_step, 0)

    for copy in first:
        copy.wait_send()
    for d in range(1, chips):
        k = lax.rem(z + d, chips) * 2 + c
        forward(k, d).wait_send()

    def drain(k, carry):
        for p in range(1, ep):
            e = lax.rem(g + p, ep)
            remote(
                sent.at[k, e], inc.at[k, e], b_send.at[k, e], b_recv.at[k, e], e, t
            ).wait_send()
        return carry

    lax.fori_loop(0, tp, drain, 0)


def on_device(
    tokens,
    norm_gain,
    norm_shift,
    expert_ids,
    affinity,
    expert_gate,
    expert_up,
    expert_down,
    shared_gate,
    shared_up,
    shared_down,
):
    ep = lax.axis_size("ep")
    tp = lax.axis_size("tp")
    tp_index = lax.axis_index("tp")
    rows, feat = tokens.shape
    width = feat * tp
    top_count = expert_ids.shape[1]
    block = rows // tp
    expert_count = ep * tp
    slot_cap = max(1, 2 * block * top_count // expert_count)
    slots = tp * slot_cap
    hid = expert_gate.shape[2]
    shared_rows = shared_gate.shape[0]
    cols = 256
    chunks = width // cols
    chips = tp // 2

    weights = affinity / jnp.sum(affinity, axis=1, keepdims=True) * ROUTED_SCALE
    experts = jnp.arange(ep, dtype=jnp.int32) * tp + tp_index
    hits = expert_ids[:, None, :] == experts[None, :, None]
    chosen = jnp.any(hits, axis=2)
    pair_weight = jnp.sum(jnp.where(hits, weights[:, None, :], 0), axis=2)
    order = jnp.arange(rows, dtype=jnp.int32)
    before = (order[:, None] > order[None, :]) & (
        order[:, None] // block == order[None, :] // block
    )
    ranks = jnp.dot(
        before.astype(BF16), chosen.astype(BF16), preferred_element_type=F32
    ).astype(jnp.int32)
    base = (order // block)[:, None] * slot_cap + jnp.arange(ep, dtype=jnp.int32)[None, :] * slots
    place = jnp.where(chosen, base + ranks, -1)

    vmem = pl.BlockSpec(memory_space=pltpu.VMEM)
    anywhere = pl.BlockSpec(memory_space=pl.ANY)
    dma = pltpu.SemaphoreType.DMA
    return pl.pallas_call(
        functools.partial(layer_kernel, (ep, tp, rows, slots, feat, chunks, cols)),
        out_shape=jax.ShapeDtypeStruct((block, width), BF16),
        in_specs=[vmem] * 8 + [anywhere] * 4,
        out_specs=vmem,
        scratch_shapes=[
            pltpu.VMEM((width, hid), BF16),
            pltpu.VMEM((width, hid), BF16),
            pltpu.VMEM((hid, width), BF16),
            pltpu.VMEM((shared_rows, width), BF16),
            pltpu.VMEM((tp, rows, feat), BF16),
            pltpu.VMEM((ep, slots, rows), BF16),
            pltpu.VMEM((rows, ep * slots), BF16),
            pltpu.VMEM((tp, ep, slots, feat), BF16),
            pltpu.VMEM((tp, ep, slots, feat), BF16),
            pltpu.VMEM((max(rows, slots), width), BF16),
            pltpu.VMEM((ep, slots, hid), BF16),
            pltpu.VMEM((rows, shared_rows), BF16),
            pltpu.VMEM((chunks, ep, slots, cols), BF16),
            pltpu.VMEM((chunks, ep, slots, cols), BF16),
            pltpu.VMEM((tp, block, cols), F32),
            pltpu.VMEM((chunks, block, cols), F32),
            pltpu.VMEM((chunks, chips, block, cols), BF16),
            pltpu.VMEM((chunks, chips, block, cols), BF16),
            pltpu.VMEM((chunks, chips, block, cols), BF16),
            pltpu.VMEM((chunks, chips, block, cols), BF16),
            dma((4,)),
            dma((chips,)),
            dma((chips,)),
            dma((tp,)),
            dma((tp, ep)),
            dma((tp, ep)),
            dma((chunks, ep)),
            dma((chunks, ep)),
            dma((chunks,)),
            dma((chunks,)),
            dma((chunks, chips)),
            dma((chunks, chips)),
        ],
        compiler_params=pltpu.CompilerParams(
            collective_id=0, has_side_effects=True, vmem_limit_bytes=56 * 1024 * 1024
        ),
        name="moe_layer",
    )(
        tokens,
        place,
        place.T,
        pair_weight,
        norm_gain.reshape(1, width),
        norm_shift.reshape(1, width),
        shared_gate,
        shared_up,
        expert_gate[0],
        expert_up[0],
        expert_down[0],
        shared_down,
    )


def solution(mesh):
    placed = (
        P("ep", "tp"),
        P(),
        P(),
        P("ep", None),
        P("ep", None),
        P(("ep", "tp"), None, None),
        P(("ep", "tp"), None, None),
        P(("ep", "tp"), None, None),
        P("tp", None),
        P("tp", None),
        P(),
    )
    return jax.shard_map(
        on_device, mesh=mesh, in_specs=placed, out_specs=P(("ep", "tp"), None), check_vma=False
    )
```

time: 196 us -> 113 us (0.58)
  Pallas kernels: 0 us -> 105 us
  waiting for transfers between devices: 103 us -> 0 us
  blocking collectives: 40.5 us -> 0 us
  matrix products: 27.1 us -> 0.33 us
  between operations: 13.5 us -> 0.02 us
  starting transfers between devices: 4.81 us -> 0 us
    pallas_call x0 -> x1, Pallas kernels: none -> 105 us  [on_device(): pl.pallas_call(functools.partial(layer_kernel, (ep, tp, rows, slots, feat...]
    all_to_all x1 -> x0, blocking collectives: 40.5 us -> none  [on_device(): lax.all_to_all(outgoing, 'ep', split_axis=0, concat_axis=0, tiled=True)]
    reduce_scatter x1 -> x0, waiting for transfers between devices: 35.9 us -> none  [on_device(): lax.psum_scatter(part.astype(jnp.bfloat16), 'tp', scatter_dimension=0, ti...]
    all_gather x1 -> x0, waiting for transfers between devices: 33.5 us -> none  [on_device(): whole = lax.all_gather(tokens, 'tp', axis=1, tiled=True)]
    all_to_all x1 -> x0, waiting for transfers between devices: 32.8 us -> none  [on_device(): lax.all_to_all(result.reshape(incoming.shape), 'ep', split_axis=0, concat...]
    dot_general x7 -> x1, matrix products: 27.1 us -> 0.33 us  [on_device(): jnp.dot(before.astype(BF16), chosen.astype(BF16), preferred_element_type=...]
    all_to_all x1 -> x0, starting transfers between devices: 4.77 us -> none  [on_device(): lax.all_to_all(result.reshape(incoming.shape), 'ep', split_axis=0, concat...]
    reduce_sum x2 -> x0, other arithmetic: 2.77 us -> none  [the longest x1 2.09 us: on_device(): center = values - jnp.mean(values, axis=1, keepdims=True)]
  transfers between devices with their start and end apart: 3 -> 0, of which waited for: 3 -> 0; matrix products, arithmetic and copies ran while one was open for 2% -> 0% of each run, Pallas kernels for 0% -> 0%
where the time goes in v2:
time: 113 us; the launch traced here: 112 us
  Pallas kernels  105 us (93%)
  other arithmetic  3.76 us (3%)
  local copies, waits for them, and re-layouts  3.38 us (3%)
    pallas_call x1, Pallas kernels, on_device(): pl.pallas_call(functools.partial(layer_kernel, (ep, tp, rows, slots, feat...  105 us

profile of v2, /device:TPU:0, one launch (start us, length us, event | category | flops | bytes accessed | tf_op | source)
XLA Modules:
  0.0 112.0 jit_solution(3880794116353952802)
XLA Ops:
  0.0 0.8 compare_reduce_fusion
  0.8 0.7 reduce_sum.18
  1.6 0.7 divide_multiply_fusion
  2.3 0.8 fusion.5
  3.1 0.3 add_select_fusion
  3.4 0.7 fusion.6.slot_t_ref
  4.1 0.9 copy.15.slot_ref
  5.0 0.8 copy.16.weight_ref
  5.8 104.6 %moe_layer.1 = bf16[64,2048]{1,0:T(8,128)(2,1)} custom-call(bf16[512,256]{1,0:T(8,128)(2,1)} %tokens_ref.1, s32[512,4]{1,0:T(8,128)} %copy.15.slot_ref, s32[4,512]{1,0:T(4,128)} %fusion.6.slot_t_ref, f32[512,4]{1,0:T(8,128)} %copy.16.weight_ref, f32[1,2048]{1,0:T(1,128)} %bitcast.15, f32[1,2048]{1,0:T(1,128)} %bitcast.16, bf16[64,2048]{1,0:T(8,128)(2,1)} %sgate_ref.1, ...), custom_call_target="tpu_custom_call" | custom-call | tf_op jit(solution)/shard_map/moe_layer/pallas_call | solution.py:348
  110.4 1.7 %copy.18 = bf16[64,2048]{1,0:T(8,128)(2,1)} copy(bf16[64,2048]{1,0:T(8,128)(2,1)} %moe_layer.1) | data formatting | bytes 524288
  (3 shorter events, 0.0 us)

commit v3 on v2

--- a/solution.py
+++ b/solution.py
@@ -15,12 +15,21 @@
 BF16 = jnp.bfloat16
 
 
+def partner(index, step, count):
+    if count & (count - 1):
+        return lax.rem(index + step, count)
+    result, bit = 0, 1
+    while bit < count:
+        result = result + ((index // bit) % 2 + (step // bit) % 2) % 2 * bit
+        bit *= 2
+    return result
+
+
 def layer_kernel(
     sizes,
     tokens_ref,
-    slot_ref,
-    slot_t_ref,
-    weight_ref,
+    ids_ref,
+    affinity_ref,
     gain_ref,
     shift_ref,
     sgate_ref,
@@ -36,6 +45,7 @@
     sdown_ref,
     whole,
     pick,
+    spread_t,
     spread,
     sent,
     inc,
@@ -63,7 +73,7 @@
     q_send,
     q_recv,
 ):
-    ep, tp, rows, slots, feat, chunks, cols = sizes
+    ep, tp, rows, slots, slot_cap, feat, chunks, cols = sizes
     chips = tp // 2
     g = lax.axis_index("ep")
     t = lax.axis_index("tp")
@@ -97,39 +107,61 @@
         )
 
     barrier = pltpu.get_barrier_semaphore()
-    partners = [(lax.rem(g + p, ep), t) for p in range(1, ep)]
-    partners += [(g, lax.rem(z + d, chips) * 2 + c) for d in range(1, chips)]
+    partners = [(partner(g, p, ep), t) for p in range(1, ep)]
+    partners += [(g, partner(z, d, chips) * 2 + c) for d in range(1, chips)]
     partners += [(g, mate)]
     for e, k in partners:
         pl.semaphore_signal(barrier, inc=1, device_id=(e, k), device_id_type=MESH)
+    ids = ids_ref[...]
+    affinity = affinity_ref[...]
+    weights = affinity / jnp.sum(affinity, axis=0, keepdims=True) * ROUTED_SCALE
+    block = rows // tp
+    early = lax.broadcasted_iota(jnp.int32, (rows, rows), 0)
+    late = lax.broadcasted_iota(jnp.int32, (rows, rows), 1)
+    before = jnp.where((early < late) & (early // block == late // block), 1.0, 0.0).astype(BF16)
+    hits = [ids == e * tp + t for e in range(ep)]
+    chosen = [jnp.sum(jnp.where(hit, 1.0, 0.0), axis=0, keepdims=True) for hit in hits]
+    pad = [jnp.zeros((-ep % 16, rows), F32)] if ep % 16 else []
+    ranks = jnp.dot(
+        jnp.concatenate(chosen + pad, axis=0).astype(BF16), before, preferred_element_type=F32
+    ).astype(jnp.int32)
+    base = lax.broadcasted_iota(jnp.int32, (1, rows), 1) // block * slot_cap
+    line = lax.broadcasted_iota(jnp.int32, (slots, rows), 0)
+    for e in range(ep):
+        place = jnp.where(chosen[e] > 0.5, base + ranks[e : e + 1, :], -1)
+        weight = jnp.sum(jnp.where(hits[e], weights, 0.0), axis=0, keepdims=True)
+        pick[e] = jnp.where(line == place, 1.0, 0.0).astype(BF16)
+        spread_t[pl.ds(e * slots, slots), :] = jnp.where(line == place, weight, 0.0)
     pl.semaphore_wait(barrier, len(partners))
 
     first = []
     first.append(remote(tokens_ref, whole.at[t], f_send.at[0], a_recv.at[t], g, mate))
     for d in range(1, chips):
-        there = lax.rem(z + d, chips) * 2 + c
+        there = partner(z, d, chips) * 2 + c
         first.append(remote(tokens_ref, whole.at[t], a_send.at[d], a_recv.at[t], g, there))
     for copy in first:
         copy.start()
     whole[t] = tokens_ref[...]
 
-    for e in range(ep):
-        line = lax.broadcasted_iota(jnp.int32, (slots, rows), 0) + e * slots
-        pick[e] = jnp.where(line == slot_t_ref[e : e + 1, :], 1.0, 0.0).astype(BF16)
-    line = lax.broadcasted_iota(jnp.int32, (rows, ep * slots), 1)
-    mixed = jnp.zeros((rows, ep * slots), F32)
-    for e in range(ep):
-        mixed = jnp.where(line == slot_ref[:, e : e + 1], weight_ref[:, e : e + 1], mixed)
-    spread[...] = mixed.astype(BF16)
-
     def forward(k, d):
         return remote(whole.at[k], whole.at[k], f_send.at[d], a_recv.at[k], g, mate)
 
-    def chunk_step(i, carry):
+    def chunk_at(i):
         d = i // 2
         side = i % 2
-        zz = lax.rem(z + d, chips)
-        k = zz * 2 + lax.rem(c + side, 2)
+        return d, side, partner(z, d, chips) * 2 + lax.rem(c + side, 2)
+
+    near = [p for p in range(1, ep) if not p & (p - 1)]
+    far = [p for p in range(1, ep) if p & (p - 1)]
+    lag = tp // 2
+    half = chunks // 2
+
+    def send_rows(k, p):
+        e = partner(g, p, ep)
+        remote(sent.at[k, e], inc.at[k, g], b_send.at[k, e], b_recv.at[k, g], e, t).start()
+
+    def chunk_step(i, carry):
+        d, side, k = chunk_at(i)
 
         @pl.when(i > 0)
         def _():
@@ -144,14 +176,27 @@
         ).astype(BF16)
         sent[k] = picked.reshape(ep, slots, feat)
         inc[k, g] = sent[k, g]
-        for p in range(1, ep):
-            e = lax.rem(g + p, ep)
-            remote(
-                sent.at[k, e], inc.at[k, g], b_send.at[k, e], b_recv.at[k, g], e, t
-            ).start()
+        for p in near:
+            send_rows(k, p)
+        if far:
+
+            @pl.when(i >= lag)
+            def _():
+                for p in far:
+                    send_rows(chunk_at(i - lag)[2], p)
+
         return carry
 
     lax.fori_loop(0, tp, chunk_step, 0)
+
+    def late_step(i, carry):
+        for p in far:
+            send_rows(chunk_at(i)[2], p)
+        return carry
+
+    if far:
+        lax.fori_loop(tp - lag, tp, late_step, 0)
+    spread[...] = spread_t[...].T.astype(BF16)
 
     def normalise(read, count):
         tile = math.gcd(64, count)
@@ -186,7 +231,7 @@
         load.wait()
 
     def expert_step(p, carry):
-        s = lax.rem(g + p, ep)
+        s = partner(g, p, ep)
 
         @pl.when(p > 0)
         def _():
@@ -200,26 +245,50 @@
         gate_act = jnp.dot(got, gate_ref[...], preferred_element_type=F32)
         up_act = jnp.dot(got, up_ref[...], preferred_element_type=F32)
         hidden[s] = (jax.nn.silu(gate_act) * up_act).astype(BF16)
-        return carry
-
-    lax.fori_loop(0, ep, expert_step, 0)
+
+        @pl.when(p == 0)
+        def _():
+            def own_step(i, carry):
+                ret[i, g] = down_rows(i, g)
+                return carry
+
+            lax.fori_loop(0, chunks, own_step, 0)
+
+        is_near = functools.reduce(jnp.logical_or, [p == n for n in near])
+
+        @pl.when(is_near)
+        def _():
+            def near_step(i, carry):
+                send_result(i, s)
+                return carry
+
+            lax.fori_loop(0, half, near_step, 0)
+
+        return carry
 
     def lanes_of(i):
         return pl.ds(pl.multiple_of(i * cols, cols), cols)
 
+    def down_rows(i, s):
+        return jnp.dot(
+            hidden[s], down_ref[:, lanes_of(i)], preferred_element_type=F32
+        ).astype(BF16)
+
+    def send_result(i, s):
+        res[i, s] = down_rows(i, s)
+        remote(res.at[i, s], ret.at[i, g], r_send.at[i, s], r_recv.at[i, g], s, t).start()
+
+    lax.fori_loop(0, ep, expert_step, 0)
+
     def down_step(i, carry):
-        rows_out = jnp.dot(
-            hidden[...].reshape(ep * slots, hidden.shape[2]),
-            down_ref[:, lanes_of(i)],
-            preferred_element_type=F32,
-        ).astype(BF16)
-        res[i] = rows_out.reshape(ep, slots, cols)
-        ret[i, g] = res[i, g]
-        for p in range(1, ep):
-            e = lax.rem(g + p, ep)
-            remote(
-                res.at[i, e], ret.at[i, g], r_send.at[i, e], r_recv.at[i, g], e, t
-            ).start()
+        for p in far:
+            send_result(i, partner(g, p, ep))
+
+        @pl.when(i < chunks - half)
+        def _():
+            for p in near:
+                send_result(i + half, partner(g, p, ep))
+
         return carry
 
     lax.fori_loop(0, chunks, down_step, 0)
@@ -227,24 +296,25 @@
     def pair_copy(i):
         return remote(pair_out.at[i], pair_in.at[i], p_send.at[i], p_recv.at[i], g, mate)
 
-    def sum_step(i, carry):
+    def produce(i):
         for p in range(1, ep):
-            s = lax.rem(g + p, ep)
+            s = partner(g, p, ep)
             remote(
                 res.at[i, s], ret.at[i, s], r_send.at[i, s], r_recv.at[i, s], s, t
             ).wait_recv()
         total = jnp.dot(
             spread[...], ret[i].reshape(ep * slots, cols), preferred_element_type=F32
         ) + jnp.dot(shidden[...], sdown_ref[:, lanes_of(i)], preferred_element_type=F32)
-        part[...] = total.reshape(part.shape)
+        part[i % 2] = total.reshape(part.shape[1:])
         for zz in range(chips):
-            pair_out[i, zz] = part[zz * 2 + 1 - c].astype(BF16)
+            pair_out[i, zz] = part[i % 2, zz * 2 + 1 - c].astype(BF16)
         pair_copy(i).start()
+
+    def finish(i):
         pair_copy(i).wait_recv()
-        own[i] = part[t] + pair_in[i, z].astype(F32)
         for d in range(1, chips):
-            zz = lax.rem(z + d, chips)
-            far_out[i, zz] = (part[zz * 2 + c] + pair_in[i, zz].astype(F32)).astype(BF16)
+            zz = partner(z, d, chips)
+            far_out[i, zz] = (part[i % 2, zz * 2 + c] + pair_in[i, zz].astype(F32)).astype(BF16)
             remote(
                 far_out.at[i, zz],
                 far_in.at[i, z],
@@ -253,14 +323,25 @@
                 g,
                 zz * 2 + c,
             ).start()
-        return carry
-
-    lax.fori_loop(0, chunks, sum_step, 0)
+        own[i] = part[i % 2, t] + pair_in[i, z].astype(F32)
+
+    def sum_step(i, carry):
+        @pl.when(i < chunks)
+        def _():
+            produce(i)
+
+        @pl.when(i > 0)
+        def _():
+            finish(i - 1)
+
+        return carry
+
+    lax.fori_loop(0, chunks + 1, sum_step, 0)
 
     def out_step(i, carry):
         total = own[i]
         for d in range(1, chips):
-            zz = lax.rem(z + d, chips)
+            zz = partner(z, d, chips)
             remote(
                 far_out.at[i, zz],
                 far_in.at[i, zz],
@@ -273,7 +354,7 @@
         out_ref[:, lanes_of(i)] = total.astype(BF16)
         pair_copy(i).wait_send()
         for p in range(1, ep):
-            e = lax.rem(g + p, ep)
+            e = partner(g, p, ep)
             remote(
                 res.at[i, e], ret.at[i, e], r_send.at[i, e], r_recv.at[i, e], e, t
             ).wait_send()
@@ -284,12 +365,12 @@
     for copy in first:
         copy.wait_send()
     for d in range(1, chips):
-        k = lax.rem(z + d, chips) * 2 + c
+        k = partner(z, d, chips) * 2 + c
         forward(k, d).wait_send()
 
     def drain(k, carry):
         for p in range(1, ep):
-            e = lax.rem(g + p, ep)
+            e = partner(g, p, ep)
             remote(
                 sent.at[k, e], inc.at[k, e], b_send.at[k, e], b_recv.at[k, e], e, t
             ).wait_send()
@@ -313,7 +394,6 @@
 ):
     ep = lax.axis_size("ep")
     tp = lax.axis_size("tp")
-    tp_index = lax.axis_index("tp")
     rows, feat = tokens.shape
     width = feat * tp
     top_count = expert_ids.shape[1]
@@ -327,28 +407,13 @@
     chunks = width // cols
     chips = tp // 2
 
-    weights = affinity / jnp.sum(affinity, axis=1, keepdims=True) * ROUTED_SCALE
-    experts = jnp.arange(ep, dtype=jnp.int32) * tp + tp_index
-    hits = expert_ids[:, None, :] == experts[None, :, None]
-    chosen = jnp.any(hits, axis=2)
-    pair_weight = jnp.sum(jnp.where(hits, weights[:, None, :], 0), axis=2)
-    order = jnp.arange(rows, dtype=jnp.int32)
-    before = (order[:, None] > order[None, :]) & (
-        order[:, None] // block == order[None, :] // block
-    )
-    ranks = jnp.dot(
-        before.astype(BF16), chosen.astype(BF16), preferred_element_type=F32
-    ).astype(jnp.int32)
-    base = (order // block)[:, None] * slot_cap + jnp.arange(ep, dtype=jnp.int32)[None, :] * slots
-    place = jnp.where(chosen, base + ranks, -1)
-
     vmem = pl.BlockSpec(memory_space=pltpu.VMEM)
     anywhere = pl.BlockSpec(memory_space=pl.ANY)
     dma = pltpu.SemaphoreType.DMA
     return pl.pallas_call(
-        functools.partial(layer_kernel, (ep, tp, rows, slots, feat, chunks, cols)),
+        functools.partial(layer_kernel, (ep, tp, rows, slots, slot_cap, feat, chunks, cols)),
         out_shape=jax.ShapeDtypeStruct((block, width), BF16),
-        in_specs=[vmem] * 8 + [anywhere] * 4,
+        in_specs=[vmem] * 7 + [anywhere] * 4,
         out_specs=vmem,
         scratch_shapes=[
             pltpu.VMEM((width, hid), BF16),
@@ -357,6 +422,7 @@
             pltpu.VMEM((shared_rows, width), BF16),
             pltpu.VMEM((tp, rows, feat), BF16),
             pltpu.VMEM((ep, slots, rows), BF16),
+            pltpu.VMEM((ep * slots, rows), F32),
             pltpu.VMEM((rows, ep * slots), BF16),
             pltpu.VMEM((tp, ep, slots, feat), BF16),
             pltpu.VMEM((tp, ep, slots, feat), BF16),
@@ -365,7 +431,7 @@
             pltpu.VMEM((rows, shared_rows), BF16),
             pltpu.VMEM((chunks, ep, slots, cols), BF16),
             pltpu.VMEM((chunks, ep, slots, cols), BF16),
-            pltpu.VMEM((tp, block, cols), F32),
+            pltpu.VMEM((2, tp, block, cols), F32),
             pltpu.VMEM((chunks, block, cols), F32),
             pltpu.VMEM((chunks, chips, block, cols), BF16),
             pltpu.VMEM((chunks, chips, block, cols), BF16),
@@ -390,9 +456,8 @@
         name="moe_layer",
     )(
         tokens,
-        place,
-        place.T,
-        pair_weight,
+        expert_ids.T,
+        affinity.T,
         norm_gain.reshape(1, width),
         norm_shift.reshape(1, width),
         shared_gate,

time: 113 us -> 100 us (0.88)
  Pallas kernels: 105 us -> 98.4 us
  other arithmetic: 3.76 us -> 0 us
  local copies, waits for them, and re-layouts: 3.38 us -> 1.67 us
    pallas_call x1, Pallas kernels: 105 us -> 98.4 us  [on_device(): pl.pallas_call(functools.partial(layer_kernel, (ep, tp, rows, slots, slot...]
    reduce_sum x2 -> x0, other arithmetic: 1.55 us -> none  [the longest x1 0.81 us: on_device(): pair_weight = jnp.sum(jnp.where(hits, weights[:, None, :], 0), axis=2)]
where the time goes in v3:
time: 100 us
  Pallas kernels  98.4 us (98%)
  local copies, waits for them, and re-layouts  1.67 us (2%)
    pallas_call x1, Pallas kernels, on_device(): pl.pallas_call(functools.partial(layer_kernel, (ep, tp, rows, slots, slot...  98.4 us

profile of v3, /device:TPU:0, one launch (start us, length us, event | category | flops | bytes accessed | tf_op | source)
XLA Modules:
  0.0 100.1 jit_solution(7337550701589458970)
XLA Ops:
  0.0 98.4 %moe_layer.1 = bf16[64,2048]{1,0:T(8,128)(2,1)} custom-call(bf16[512,256]{1,0:T(8,128)(2,1)} %tokens_ref.1, s32[6,512]{1,0:T(8,128)} %bitcast.10, f32[6,512]{1,0:T(8,128)} %bitcast.11, f32[1,2048]{1,0:T(1,128)} %bitcast.12, f32[1,2048]{1,0:T(1,128)} %bitcast.13, bf16[64,2048]{1,0:T(8,128)(2,1)} %sgate_ref.1, bf16[64,2048]{1,0:T(8,128)(2,1)} %sup_ref.1, ...), custom_call_target="tpu_custom_call" | custom-call | tf_op jit(solution)/shard_map/moe_layer/pallas_call | solution.py:413
  98.4 1.7 %copy.13 = bf16[64,2048]{1,0:T(8,128)(2,1)} copy(bf16[64,2048]{1,0:T(8,128)(2,1)} %moe_layer.1) | data formatting | bytes 524288

commit v4 on v3

--- a/solution.py
+++ b/solution.py
@@ -153,12 +153,12 @@
 
     near = [p for p in range(1, ep) if not p & (p - 1)]
     far = [p for p in range(1, ep) if p & (p - 1)]
-    lag = tp // 2
-    half = chunks // 2
+    lag = 3 * tp // 8
+    half = chunks // 8
 
     def send_rows(k, p):
         e = partner(g, p, ep)
-        remote(sent.at[k, e], inc.at[k, g], b_send.at[k, e], b_recv.at[k, g], e, t).start()
+        remote(sent.at[k, e], inc.at[k, g], b_send, b_recv.at[g], e, t).start()
 
     def chunk_step(i, carry):
         d, side, k = chunk_at(i)
@@ -235,10 +235,7 @@
 
         @pl.when(p > 0)
         def _():
-            for k in range(tp):
-                remote(
-                    sent.at[k, s], inc.at[k, s], b_send.at[k, s], b_recv.at[k, s], s, t
-                ).wait_recv()
+            remote(sent.at[:, s], inc.at[:, s], b_send, b_recv.at[s], s, t).wait_recv()
 
         normalise(lambda k, at: inc[k, s, at, :], slots)
         got = norm[0:slots, :]
@@ -276,7 +273,7 @@
 
     def send_result(i, s):
         res[i, s] = down_rows(i, s)
-        remote(res.at[i, s], ret.at[i, g], r_send.at[i, s], r_recv.at[i, g], s, t).start()
+        remote(res.at[i, s], ret.at[i, g], r_send, r_recv.at[i], s, t).start()
 
     lax.fori_loop(0, ep, expert_step, 0)
 
@@ -294,14 +291,11 @@
     lax.fori_loop(0, chunks, down_step, 0)
 
     def pair_copy(i):
-        return remote(pair_out.at[i], pair_in.at[i], p_send.at[i], p_recv.at[i], g, mate)
+        return remote(pair_out.at[i], pair_in.at[i], p_send, p_recv.at[i], g, mate)
 
     def produce(i):
-        for p in range(1, ep):
-            s = partner(g, p, ep)
-            remote(
-                res.at[i, s], ret.at[i, s], r_send.at[i, s], r_recv.at[i, s], s, t
-            ).wait_recv()
+        others = pl.ds(0, ep - 1)
+        remote(res.at[i, others], ret.at[i, others], r_send, r_recv.at[i], g, mate).wait_recv()
         total = jnp.dot(
             spread[...], ret[i].reshape(ep * slots, cols), preferred_element_type=F32
         ) + jnp.dot(shidden[...], sdown_ref[:, lanes_of(i)], preferred_element_type=F32)
@@ -318,8 +312,8 @@
             remote(
                 far_out.at[i, zz],
                 far_in.at[i, z],
-                q_send.at[i, zz],
-                q_recv.at[i, z],
+                q_send,
+                q_recv,
                 g,
                 zz * 2 + c,
             ).start()
@@ -338,45 +332,27 @@
 
     lax.fori_loop(0, chunks + 1, sum_step, 0)
 
+    rest = pl.ds(0, chips - 1)
+    remote(far_out.at[:, rest], far_in.at[:, rest], q_send, q_recv, g, mate).wait()
+
     def out_step(i, carry):
         total = own[i]
         for d in range(1, chips):
-            zz = partner(z, d, chips)
-            remote(
-                far_out.at[i, zz],
-                far_in.at[i, zz],
-                q_send.at[i, zz],
-                q_recv.at[i, zz],
-                g,
-                zz * 2 + c,
-            ).wait()
-            total = total + far_in[i, zz].astype(F32)
+            total = total + far_in[i, partner(z, d, chips)].astype(F32)
         out_ref[:, lanes_of(i)] = total.astype(BF16)
-        pair_copy(i).wait_send()
-        for p in range(1, ep):
-            e = partner(g, p, ep)
-            remote(
-                res.at[i, e], ret.at[i, e], r_send.at[i, e], r_recv.at[i, e], e, t
-            ).wait_send()
         return carry
 
     lax.fori_loop(0, chunks, out_step, 0)
 
+    others = pl.ds(0, ep - 1)
+    remote(sent.at[:, others], inc.at[:, others], b_send, b_recv.at[g], g, mate).wait_send()
+    remote(res.at[:, others], ret.at[:, others], r_send, r_recv.at[0], g, mate).wait_send()
+    remote(pair_out, pair_in, p_send, p_recv.at[0], g, mate).wait_send()
     for copy in first:
         copy.wait_send()
     for d in range(1, chips):
         k = partner(z, d, chips) * 2 + c
         forward(k, d).wait_send()
-
-    def drain(k, carry):
-        for p in range(1, ep):
-            e = partner(g, p, ep)
-            remote(
-                sent.at[k, e], inc.at[k, e], b_send.at[k, e], b_recv.at[k, e], e, t
-            ).wait_send()
-        return carry
-
-    lax.fori_loop(0, tp, drain, 0)
 
 
 def on_device(
@@ -441,14 +417,14 @@
             dma((chips,)),
             dma((chips,)),
             dma((tp,)),
-            dma((tp, ep)),
-            dma((tp, ep)),
-            dma((chunks, ep)),
-            dma((chunks, ep)),
+            dma,
+            dma((ep,)),
+            dma,
             dma((chunks,)),
+            dma,
             dma((chunks,)),
-            dma((chunks, chips)),
-            dma((chunks, chips)),
+            dma,
+            dma,
         ],
         compiler_params=pltpu.CompilerParams(
             collective_id=0, has_side_effects=True, vmem_limit_bytes=56 * 1024 * 1024

time: 100 us -> 96.1 us (0.961)
  Pallas kernels: 98.4 us -> 94.3 us
    pallas_call x1, Pallas kernels: 98.4 us -> 94.3 us  [on_device(): pl.pallas_call(functools.partial(layer_kernel, (ep, tp, rows, slots, slot...]
where the time goes in v4:
time: 96.1 us; the launch traced here: 96 us
  Pallas kernels  94.3 us (98%)
  local copies, waits for them, and re-layouts  1.67 us (2%)
    pallas_call x1, Pallas kernels, on_device(): pl.pallas_call(functools.partial(layer_kernel, (ep, tp, rows, slots, slot...  94.3 us

profile of v4, /device:TPU:0, one launch (start us, length us, event | category | flops | bytes accessed | tf_op | source)
XLA Modules:
  0.0 96.0 jit_solution(14248648144517472797)
XLA Ops:
  0.0 94.3 %moe_layer.1 = bf16[64,2048]{1,0:T(8,128)(2,1)} custom-call(bf16[512,256]{1,0:T(8,128)(2,1)} %tokens_ref.1, s32[6,512]{1,0:T(8,128)} %bitcast.10, f32[6,512]{1,0:T(8,128)} %bitcast.11, f32[1,2048]{1,0:T(1,128)} %bitcast.12, f32[1,2048]{1,0:T(1,128)} %bitcast.13, bf16[64,2048]{1,0:T(8,128)(2,1)} %sgate_ref.1, bf16[64,2048]{1,0:T(8,128)(2,1)} %sup_ref.1, ...), custom_call_target="tpu_custom_call" | custom-call | tf_op jit(solution)/shard_map/moe_layer/pallas_call | solution.py:389
  94.3 1.7 %copy.13 = bf16[64,2048]{1,0:T(8,128)(2,1)} copy(bf16[64,2048]{1,0:T(8,128)(2,1)} %moe_layer.1) | data formatting | bytes 524288
